TPU v7x, 512 devices: a 4x2x32 block of a 4x8x32 slice. The times are simulated.
512 devices in a mesh: grp: 2 (over y), sp: 64 (over z, core), tp: 4 (over x).
Axes of the slice: x: 4, y: 2, z: 32, core: 2. Of those that a mesh axis runs over, the one named last changes fastest.
The devices are a block of a 4x8x32 slice.
Arguments:
- tokens: bfloat16 [131072, 2048], P(('grp', 'sp', 'tp')), parts along dimension 0, may hold values from -6 to 6
- step: float32 [131072], P(('grp', 'sp')), parts along dimension 0, may hold values from 0.2 to 3.75
- in_gain: float32 [2048], replicated, may hold values from 0.1 to 1.9
- in_proj: bfloat16 [2048, 512], P(None, 'tp'), may hold values from -0.125 to 0.125
- decay_rate: float32 [32, 64], P('tp'), may hold values from 1.5258789e-06 to 0.04
- frequency: float32 [32, 64], P('tp'), may hold values from 0.2 to 3
- input_map: float32 [2, 32, 64, 16], P(None, 'tp'), may hold values from -1 to 1
- readout: float32 [2, 32, 16, 64], P(None, 'tp'), may hold values from -0.75 to 0.75
- out_gain: float32 [512], replicated, may hold values from 0.1 to 1.9
- out_proj: bfloat16 [512, 2048], replicated, may hold values from -0.25 to 0.25
Outputs:
- mixed: bfloat16 [131072, 2048], P(('grp', 'sp', 'tp')), parts along dimension 0
There are 2 independent parts, one for each index of `grp`. A program takes and returns all parts, laid end to end along the dimension named above; an argument that names none is the same for every part. Nothing has to cross between parts.
All inputs are finite; a program needn't handle non-finite values.
Results may differ from a plain program's by a relative error of at most 0.01.
Values may be sent and summed in bfloat16 or wider, within the bound.
No kernel may reach another device: no remote copies, remote signals or barrier semaphores. Data moves between devices by JAX's collectives and lax.ppermute only.
A program may use at most 64 MiB of HBM per device.

v0:
```python
from functools import partial
import jax
import jax.numpy as jnp
from jax import lax
from jax.sharding import PartitionSpec as P

SPAN = 64
HIGHEST = lax.Precision.HIGHEST


def gathered_once(array, axis):
    leaves = jax.tree.leaves(array)
    sequence = sorted(range(len(leaves)), key=lambda k: -leaves[k].size)
    width = (1, *leaves[sequence[0]].shape)[-1]
    lines = [
        jnp.pad(leaves[k].reshape(-1), (0, -leaves[k].size % width)).reshape(-1, width)
        for k in sequence
    ]
    both, at, found = (lax.all_gather(jnp.concatenate(lines), axis), 0, {})
    for k, line in zip(sequence, lines):
        section = both[:, at : at + len(line)].reshape(len(both), -1)
        found[k] = section[:, : leaves[k].size].reshape(-1, *leaves[k].shape)
        at += len(line)
    numbers = iter(range(len(leaves)))
    return jax.tree.map(lambda _: found[next(numbers)], array)


def entering(value, axis, join, neutral):
    count, mine = (lax.axis_size(axis), lax.axis_index(axis))
    pieces = gathered_once(value, axis)
    so_far = jax.tree.map(
        lambda part, zero: jnp.full_like(part, 0) + jnp.asarray(zero, part.dtype), value, neutral
    )

    def lap(position, so_far):
        longer = join(so_far, jax.tree.map(lambda part: part[position], pieces))
        return jax.tree.map(lambda new, old: jnp.where(position < mine, new, old), longer, so_far)

    return lax.fori_loop(0, count - 1, lap, so_far)


def compose(earlier, later):
    a_re, a_im, b_re, b_im = earlier
    c_re, c_im, d_re, d_im = later
    return (
        c_re * a_re - c_im * a_im,
        c_re * a_im + c_im * a_re,
        c_re * b_re - c_im * b_im + d_re,
        c_re * b_im + c_im * b_re + d_im,
    )


def rms_rows(values, gain):
    values = values.astype(jnp.float32)
    scaled = values * lax.rsqrt(jnp.mean(values * values, axis=-1, keepdims=True) + 1e-06)
    return (scaled * gain).astype(jnp.bfloat16)


def block_tables(input_map, readout):
    groups = input_map.shape[1]
    unit = jnp.eye(groups, dtype=jnp.float32)
    push_re = jnp.einsum("gph,gk->ghkp", input_map[0], unit, precision=HIGHEST)
    push_im = jnp.einsum("gph,gk->ghkp", input_map[1], unit, precision=HIGHEST)
    read_re = jnp.einsum("ghp,gk->gpkh", readout[0], unit, precision=HIGHEST)
    read_im = jnp.einsum("ghp,gk->gpkh", readout[1], unit, precision=HIGHEST)
    inner = push_re.shape[0] * push_re.shape[1]
    flat = push_re.shape[2] * push_re.shape[3]
    return (
        push_re.reshape(inner, flat),
        push_im.reshape(inner, flat),
        read_re.reshape(flat, inner),
        read_im.reshape(flat, inner),
    )


def response(s_re, s_im, read_re, read_im):
    value = jnp.dot(s_re, read_re, precision=HIGHEST) - jnp.dot(s_im, read_im, precision=HIGHEST)
    return jax.nn.gelu(value, approximate=True).astype(jnp.bfloat16)


def advance(carry, piece, rates, freqs, tables, lower, keep):
    drive_part, time_part = piece
    push_re, push_im, read_re, read_im = tables
    own = time_part[:, None]
    magnitude = jnp.exp(-rates[None] * own)
    a_re = magnitude * jnp.cos(freqs[None] * own)
    a_im = magnitude * jnp.sin(freqs[None] * own)
    lam_re = -rates
    denom = lam_re * lam_re + freqs * freqs
    n_re = a_re - 1.0
    z_re = (n_re * lam_re + a_im * freqs) / denom
    z_im = (a_im * lam_re - n_re * freqs) / denom
    grouped = drive_part.astype(jnp.float32)
    in_re = jnp.dot(grouped, push_re, precision=HIGHEST)
    in_im = jnp.dot(grouped, push_im, precision=HIGHEST)
    i_re = z_re * in_re - z_im * in_im
    i_im = z_re * in_im + z_im * in_re
    elapsed = jnp.dot(lower, time_part, precision=HIGHEST)[:, None]
    grow = jnp.exp(rates[None] * elapsed)
    angle = freqs[None] * elapsed
    cosine = jnp.cos(angle)
    sine = jnp.sin(angle)
    w_re = grow * (cosine * i_re + sine * i_im)
    w_im = grow * (cosine * i_im - sine * i_re)
    acc_re = jnp.dot(lower, w_re, precision=HIGHEST)
    acc_im = jnp.dot(lower, w_im, precision=HIGHEST)
    shrink = jnp.exp(-rates[None] * elapsed)
    c_re = shrink * cosine
    c_im = shrink * sine
    s_re = c_re * acc_re - c_im * acc_im
    s_im = c_re * acc_im + c_im * acc_re
    d_re, d_im, e_re, e_im = carry
    full_re = s_re + c_re * e_re - c_im * e_im
    full_im = s_im + c_re * e_im + c_im * e_re
    cum_re = c_re * d_re - c_im * d_im
    cum_im = c_re * d_im + c_im * d_re
    ends = (cum_re[-1], cum_im[-1], full_re[-1], full_im[-1])
    return (ends, (cum_re, cum_im, full_re, full_im))


def on_device(
    tokens, step, in_gain, in_proj, decay_rate, frequency, input_map, readout, out_gain, out_proj
):
    normed = rms_rows(tokens, in_gain)
    rates, freqs, maps, reads = (decay_rate, frequency, input_map, readout)
    drive = jnp.dot(
        lax.all_gather(normed, "tp", axis=0, tiled=True),
        in_proj,
        preferred_element_type=jnp.float32,
    ).astype(jnp.bfloat16)
    tables = block_tables(maps, reads)
    flat_rates = rates.reshape(-1)
    flat_freqs = freqs.reshape(-1)
    seq_rows = drive.shape[0]
    block_count = seq_rows // SPAN
    drive_blocks = drive.reshape(block_count, SPAN, -1)
    time_blocks = step.reshape(block_count, SPAN)
    rows_index = lax.broadcasted_iota(jnp.int32, (SPAN, SPAN), 0)
    cols_index = lax.broadcasted_iota(jnp.int32, (SPAN, SPAN), 1)
    lower = (cols_index <= rows_index).astype(jnp.float32)
    zeros = jnp.zeros(flat_rates.shape, jnp.float32)
    ones = jnp.ones(flat_rates.shape, jnp.float32)
    start_carry = (ones, zeros, zeros, zeros)
    keep_first = "states"
    ends, stored = lax.scan(
        partial(
            advance, rates=flat_rates, freqs=flat_freqs, tables=tables, lower=lower, keep=keep_first
        ),
        start_carry,
        (drive_blocks, time_blocks),
    )
    incoming = entering(ends, "sp", compose, start_carry)
    cum_re, cum_im, full_re, full_im = stored
    width = flat_rates.shape[0]
    cum_re = cum_re.reshape(seq_rows, width)
    cum_im = cum_im.reshape(seq_rows, width)
    state_re = full_re.reshape(seq_rows, width) + cum_re * incoming[2] - cum_im * incoming[3]
    state_im = full_im.reshape(seq_rows, width) + cum_re * incoming[3] + cum_im * incoming[2]
    answer = response(state_re, state_im, tables[2], tables[3])
    gathered = lax.all_to_all(answer, "tp", split_axis=0, concat_axis=1, tiled=True)
    shaped = rms_rows(gathered, out_gain)
    return jnp.dot(shaped, out_proj, preferred_element_type=jnp.float32).astype(jnp.bfloat16)


def solution(mesh):
    placed = (
        P(("grp", "sp", "tp"), None),
        P(("grp", "sp")),
        P(),
        P(None, "tp"),
        P("tp", None),
        P("tp", None),
        P(None, "tp", None, None),
        P(None, "tp", None, None),
        P(),
        P(),
    )
    return jax.shard_map(
        on_device,
        mesh=mesh,
        in_specs=placed,
        out_specs=P(("grp", "sp", "tp"), None),
        check_vma=False,
    )
```

profile of v0, /device:TPU:33, one launch (start us, length us, event | category | flops | bytes accessed | tf_op | source)
XLA Modules:
  0.0 373.2 jit_solution(620879934638658215)
XLA Ops:
  6.6 1.7 fusion.44
  8.3 2.5 fusion.46
  15.7 85.1 %all-gather.4.cloned.1.call-done = bf16[1024,2048]{1,0:T(8,128)(2,1)} async-done(((bf16[256,2048]{1,0:T(8,128)(2,1)}), bf16[1024,2048]{1,0:T(8,128)(2,1)}) %all-gather.4.cloned.1.call-update) | async-done | bytes 4194320 | tf_op jit(solution)/shard_map/all_gather | solution.py:127
  100.8 4.3 %convolution_convert_fusion.1 = bf16[1024,128]{1,0:T(8,128)(2,1)} fusion(bf16[1024,2048]{1,0:T(8,128)(2,1)} %all-gather.4.cloned.1.call-done, bf16[2048,128]{1,0:T(8,128)(2,1)} %param.17), kind=kOutput, calls=%fused_computation.81 | convolution fusion | flops 537001984 | bytes 4980736 | tf_op jit(solution)/shard_map/dot_general | solution.py:126
  106.2 173.9 %while.48 = (s32[]{:T(128)}, f32[512]{0:T(512)S(1)}, f32[512]{0:T(512)S(1)}, f32[512]{0:T(512)}, f32[512]{0:T(512)}, /*index=5*/f32[16,64,512]{2,1,0:T(8,128)}, ...) while((s32[]{:T(128)}, f32[512]{0:T(512)S(1)}, ...), condition=%wide.wide.region_2.3_spmd.clone.clone.clone, body=%wide.wide.region_1.2_spmd.clone.clone.clone.sunk | while | flops 153889792 | bytes 4405837 | solution.py:145
  106.6 1.0 fusion.103
  110.2 2.0 convolution_bitcast_fusion.8
  112.3 3.0 add_dynamic-update-slice_fusion.3
  117.4 1.0 fusion.103
  118.5 1.0 fusion.104
  121.1 2.0 convolution_bitcast_fusion.8
  123.2 3.0 add_dynamic-update-slice_fusion.3
  128.3 1.0 fusion.103
  129.4 1.0 fusion.104
  131.9 2.0 convolution_bitcast_fusion.8
  134.1 3.0 add_dynamic-update-slice_fusion.3
  139.2 1.0 fusion.103
  140.3 1.0 fusion.104
  142.8 2.0 convolution_bitcast_fusion.8
  144.9 3.0 add_dynamic-update-slice_fusion.3
  150.1 1.0 fusion.103
  151.2 1.0 fusion.104
  153.7 2.0 convolution_bitcast_fusion.8
  155.8 3.0 add_dynamic-update-slice_fusion.3
  160.9 1.0 fusion.103
  162.1 1.0 fusion.104
  164.6 2.0 convolution_bitcast_fusion.8
  166.7 3.0 add_dynamic-update-slice_fusion.3
  171.8 1.0 fusion.103
  172.9 1.0 fusion.104
  175.5 2.0 convolution_bitcast_fusion.8
  177.6 3.0 add_dynamic-update-slice_fusion.3
  182.7 1.0 fusion.103
  183.8 1.0 fusion.104
  186.3 2.0 convolution_bitcast_fusion.8
  188.4 3.0 add_dynamic-update-slice_fusion.3
  193.6 1.0 fusion.103
  194.7 1.0 fusion.104
  197.2 2.0 convolution_bitcast_fusion.8
  199.3 3.0 add_dynamic-update-slice_fusion.3
  208.1 2.0 convolution_bitcast_fusion.8
  210.2 3.0 add_dynamic-update-slice_fusion.3
  218.9 2.0 convolution_bitcast_fusion.8
  221.0 3.0 add_dynamic-update-slice_fusion.3
  226.1 1.0 fusion.103
  229.8 2.0 convolution_bitcast_fusion.8
  231.9 3.0 add_dynamic-update-slice_fusion.3
  238.1 1.0 fusion.104
  240.7 2.0 convolution_bitcast_fusion.8
  242.8 3.0 add_dynamic-update-slice_fusion.3
  251.5 2.0 convolution_bitcast_fusion.8
  253.6 3.0 add_dynamic-update-slice_fusion.3
  258.8 1.0 fusion.103
  262.4 2.0 convolution_bitcast_fusion.8
  264.5 3.0 add_dynamic-update-slice_fusion.3
  273.3 2.0 convolution_bitcast_fusion.8
  275.4 3.0 add_dynamic-update-slice_fusion.3
  280.9 60.4 %all-gather.1 = f32[64,4,512]{2,1,0:T(4,128)S(1)} all-gather(f32[1,4,512]{2,1,0:T(4,128)S(1)} %maximum_bitcast_fusion), channel_id=2, replica_groups=mesh['grp'=2,'sp'=64,'tp'=4] {'sp'}, dimensions={0}, use_global_device_ids=true | all-gather | bytes 532480 | tf_op jit(solution)/shard_map/all_gather | solution.py:19
  341.7 5.1 %while.47 = (s32[]{:T(128)}, f32[512]{0:T(512)S(1)}, f32[512]{0:T(512)S(1)}, s32[]{:T(128)}, f32[64,512]{1,0:T(8,128)S(1)}, /*index=5*/f32[64,512]{1,0:T(8,128)S...) while((s32[]{:T(128)}, f32[512]{0:T(512)S(1)}, f32[512]{0:T(512)S(1)}, ...), condition=%wide.region_4.5_spmd.clone, body=%wide.region_3.4_spmd.clone.sunk | while | flops 6148 | bytes 32897 | solution.py:39
  346.8 4.6 %multiply_add_fusion.5 = (f32[16,64,512]{2,1,0:T(8,128)S(1)}, f32[16,64,512]{2,1,0:T(8,128)S(1)}) fusion(f32[16,64,512]{2,1,0:T(8,128)} %get-tuple-element.435, f32[16,64,512]{2,1,0:T(8,128)} %get-tuple-element.437, f32[16,64,512]{2,1,0:T(8,128)} %get-tuple-element.429, f32[512]{0:T(512)S(1)} %get-tuple-element.436, f32[512]{0:T(512)S(1)} %get-tuple-element.434, ...), kind=kLoop, calls=%fused_computation.78 | loop fusion | flops 4194304 | bytes 12587008 | tf_op jit(solution)/shard_map/add | solution.py:158
  351.4 1.8 fusion.59
  353.3 1.8 fusion.54
  355.2 9.2 %all_to_all.13 = bf16[4,256,128]{1,2,0:T(8,128)(2,1)S(1)} all-to-all(bf16[4,256,128]{1,2,0:T(8,128)(2,1)S(1)} %copy.20), channel_id=1, replica_groups=mesh['grp'=2,'sp'=64,'tp'=4] {'tp'}, dimensions={0} | all-to-all | bytes 524288 | tf_op jit(solution)/shard_map/all_to_all | solution.py:160
  364.7 1.7 convolution_convert_fusion
  (595 shorter events, 81.8 us)
Async XLA Ops:
  6.5 358.1 %copy-start = (bf16[512,2048]{1,0:T(8,128)(2,1)S(1)}, bf16[512,2048]{1,0:T(8,128)(2,1)}, u32[]{:S(2)}) copy-start(bf16[512,2048]{1,0:T(8,128)(2,1)} %param.23) | copy-start | bytes 6291460
  6.6 6.4 %copy-start.12 = (f32[1024]{0:T(1024)S(1)}, f32[1024]{0:T(1024)}, u32[]{:S(2)}) copy-start(f32[1024]{0:T(1024)} %param.15) | copy-start | bytes 12292
  6.6 7.0 %copy-start.3 = (f32[2,8,16,64]{3,2,1,0:T(8,128)S(1)}, f32[2,8,16,64]{3,2,1,0:T(8,128)}, u32[]{:S(2)}) copy-start(f32[2,8,16,64]{3,2,1,0:T(8,128)} %param.21) | copy-start | bytes 196612
  6.6 94.2 %all-gather.4.cloned.1.call-start = ((), (), s32[]{:S(2)}) async-start(), calls=%async_computation.1 | async-start | bytes 5242880 | tf_op jit(solution)/shard_map/all_gather | solution.py:127
  106.5 5.7 %copy-start.5 = (f32[1,512]{1,0:T(1,128)S(1)}, f32[1,512]{1,0:T(1,128)}, u32[]{:S(2)}) copy-start(f32[1,512]{1,0:T(1,128)} %get-tuple-element.1028) | copy-start | bytes 6148 | tf_op jit(solution)/shard_map/while
  106.5 5.7 %copy-start.10 = (f32[512]{0:T(512)S(1)}, f32[512]{0:T(512)}, u32[]{:S(2)}) copy-start(f32[512]{0:T(512)} %get-tuple-element.1001) | copy-start | bytes 6148 | tf_op jit(solution)/shard_map/while
  106.5 5.7 %copy-start.11 = (f32[512]{0:T(512)S(1)}, f32[512]{0:T(512)}, u32[]{:S(2)}) copy-start(f32[512]{0:T(512)} %get-tuple-element.1002) | copy-start | bytes 6148 | tf_op jit(solution)/shard_map/while
  106.5 5.7 %copy-start.14 = (f32[512]{0:T(512)S(1)}, f32[512]{0:T(512)}, u32[]{:S(2)}) copy-start(f32[512]{0:T(512)} %get-tuple-element.1038) | copy-start | bytes 6148 | tf_op jit(solution)/shard_map/while
  106.6 5.7 %copy-start.15 = (f32[1,512]{1,0:T(1,128)S(1)}, f32[1,512]{1,0:T(1,128)}, u32[]{:S(2)}) copy-start(f32[1,512]{1,0:T(1,128)} %get-tuple-element.1032) | copy-start | bytes 6148 | tf_op jit(solution)/shard_map/while
  117.4 5.7 %copy-start.5 = (f32[1,512]{1,0:T(1,128)S(1)}, f32[1,512]{1,0:T(1,128)}, u32[]{:S(2)}) copy-start(f32[1,512]{1,0:T(1,128)} %get-tuple-element.1028) | copy-start | bytes 6148 | tf_op jit(solution)/shard_map/while
  117.4 5.7 %copy-start.10 = (f32[512]{0:T(512)S(1)}, f32[512]{0:T(512)}, u32[]{:S(2)}) copy-start(f32[512]{0:T(512)} %get-tuple-element.1001) | copy-start | bytes 6148 | tf_op jit(solution)/shard_map/while
  128.3 5.7 %copy-start.5 = (f32[1,512]{1,0:T(1,128)S(1)}, f32[1,512]{1,0:T(1,128)}, u32[]{:S(2)}) copy-start(f32[1,512]{1,0:T(1,128)} %get-tuple-element.1028) | copy-start | bytes 6148 | tf_op jit(solution)/shard_map/while
  128.3 5.7 %copy-start.10 = (f32[512]{0:T(512)S(1)}, f32[512]{0:T(512)}, u32[]{:S(2)}) copy-start(f32[512]{0:T(512)} %get-tuple-element.1001) | copy-start | bytes 6148 | tf_op jit(solution)/shard_map/while
  128.3 5.7 %copy-start.11 = (f32[512]{0:T(512)S(1)}, f32[512]{0:T(512)}, u32[]{:S(2)}) copy-start(f32[512]{0:T(512)} %get-tuple-element.1002) | copy-start | bytes 6148 | tf_op jit(solution)/shard_map/while
  128.3 5.7 %copy-start.14 = (f32[512]{0:T(512)S(1)}, f32[512]{0:T(512)}, u32[]{:S(2)}) copy-start(f32[512]{0:T(512)} %get-tuple-element.1038) | copy-start | bytes 6148 | tf_op jit(solution)/shard_map/while
  128.3 5.7 %copy-start.15 = (f32[1,512]{1,0:T(1,128)S(1)}, f32[1,512]{1,0:T(1,128)}, u32[]{:S(2)}) copy-start(f32[1,512]{1,0:T(1,128)} %get-tuple-element.1032) | copy-start | bytes 6148 | tf_op jit(solution)/shard_map/while
  139.1 5.7 %copy-start.5 = (f32[1,512]{1,0:T(1,128)S(1)}, f32[1,512]{1,0:T(1,128)}, u32[]{:S(2)}) copy-start(f32[1,512]{1,0:T(1,128)} %get-tuple-element.1028) | copy-start | bytes 6148 | tf_op jit(solution)/shard_map/while
  139.2 5.7 %copy-start.10 = (f32[512]{0:T(512)S(1)}, f32[512]{0:T(512)}, u32[]{:S(2)}) copy-start(f32[512]{0:T(512)} %get-tuple-element.1001) | copy-start | bytes 6148 | tf_op jit(solution)/shard_map/while
  139.2 5.7 %copy-start.11 = (f32[512]{0:T(512)S(1)}, f32[512]{0:T(512)}, u32[]{:S(2)}) copy-start(f32[512]{0:T(512)} %get-tuple-element.1002) | copy-start | bytes 6148 | tf_op jit(solution)/shard_map/while
  139.2 5.7 %copy-start.14 = (f32[512]{0:T(512)S(1)}, f32[512]{0:T(512)}, u32[]{:S(2)}) copy-start(f32[512]{0:T(512)} %get-tuple-element.1038) | copy-start | bytes 6148 | tf_op jit(solution)/shard_map/while
  139.2 5.7 %copy-start.15 = (f32[1,512]{1,0:T(1,128)S(1)}, f32[1,512]{1,0:T(1,128)}, u32[]{:S(2)}) copy-start(f32[1,512]{1,0:T(1,128)} %get-tuple-element.1032) | copy-start | bytes 6148 | tf_op jit(solution)/shard_map/while
  150.0 5.7 %copy-start.5 = (f32[1,512]{1,0:T(1,128)S(1)}, f32[1,512]{1,0:T(1,128)}, u32[]{:S(2)}) copy-start(f32[1,512]{1,0:T(1,128)} %get-tuple-element.1028) | copy-start | bytes 6148 | tf_op jit(solution)/shard_map/while
  150.0 5.7 %copy-start.10 = (f32[512]{0:T(512)S(1)}, f32[512]{0:T(512)}, u32[]{:S(2)}) copy-start(f32[512]{0:T(512)} %get-tuple-element.1001) | copy-start | bytes 6148 | tf_op jit(solution)/shard_map/while
  150.0 5.7 %copy-start.11 = (f32[512]{0:T(512)S(1)}, f32[512]{0:T(512)}, u32[]{:S(2)}) copy-start(f32[512]{0:T(512)} %get-tuple-element.1002) | copy-start | bytes 6148 | tf_op jit(solution)/shard_map/while
  150.0 5.7 %copy-start.14 = (f32[512]{0:T(512)S(1)}, f32[512]{0:T(512)}, u32[]{:S(2)}) copy-start(f32[512]{0:T(512)} %get-tuple-element.1038) | copy-start | bytes 6148 | tf_op jit(solution)/shard_map/while
  150.1 5.7 %copy-start.15 = (f32[1,512]{1,0:T(1,128)S(1)}, f32[1,512]{1,0:T(1,128)}, u32[]{:S(2)}) copy-start(f32[1,512]{1,0:T(1,128)} %get-tuple-element.1032) | copy-start | bytes 6148 | tf_op jit(solution)/shard_map/while
  160.9 5.7 %copy-start.5 = (f32[1,512]{1,0:T(1,128)S(1)}, f32[1,512]{1,0:T(1,128)}, u32[]{:S(2)}) copy-start(f32[1,512]{1,0:T(1,128)} %get-tuple-element.1028) | copy-start | bytes 6148 | tf_op jit(solution)/shard_map/while
  160.9 5.7 %copy-start.10 = (f32[512]{0:T(512)S(1)}, f32[512]{0:T(512)}, u32[]{:S(2)}) copy-start(f32[512]{0:T(512)} %get-tuple-element.1001) | copy-start | bytes 6148 | tf_op jit(solution)/shard_map/while
  160.9 5.7 %copy-start.11 = (f32[512]{0:T(512)S(1)}, f32[512]{0:T(512)}, u32[]{:S(2)}) copy-start(f32[512]{0:T(512)} %get-tuple-element.1002) | copy-start | bytes 6148 | tf_op jit(solution)/shard_map/while
  160.9 5.7 %copy-start.14 = (f32[512]{0:T(512)S(1)}, f32[512]{0:T(512)}, u32[]{:S(2)}) copy-start(f32[512]{0:T(512)} %get-tuple-element.1038) | copy-start | bytes 6148 | tf_op jit(solution)/shard_map/while
  160.9 5.7 %copy-start.15 = (f32[1,512]{1,0:T(1,128)S(1)}, f32[1,512]{1,0:T(1,128)}, u32[]{:S(2)}) copy-start(f32[1,512]{1,0:T(1,128)} %get-tuple-element.1032) | copy-start | bytes 6148 | tf_op jit(solution)/shard_map/while
  171.8 5.7 %copy-start.5 = (f32[1,512]{1,0:T(1,128)S(1)}, f32[1,512]{1,0:T(1,128)}, u32[]{:S(2)}) copy-start(f32[1,512]{1,0:T(1,128)} %get-tuple-element.1028) | copy-start | bytes 6148 | tf_op jit(solution)/shard_map/while
  171.8 5.7 %copy-start.10 = (f32[512]{0:T(512)S(1)}, f32[512]{0:T(512)}, u32[]{:S(2)}) copy-start(f32[512]{0:T(512)} %get-tuple-element.1001) | copy-start | bytes 6148 | tf_op jit(solution)/shard_map/while
  171.8 5.7 %copy-start.11 = (f32[512]{0:T(512)S(1)}, f32[512]{0:T(512)}, u32[]{:S(2)}) copy-start(f32[512]{0:T(512)} %get-tuple-element.1002) | copy-start | bytes 6148 | tf_op jit(solution)/shard_map/while
  171.8 5.7 %copy-start.14 = (f32[512]{0:T(512)S(1)}, f32[512]{0:T(512)}, u32[]{:S(2)}) copy-start(f32[512]{0:T(512)} %get-tuple-element.1038) | copy-start | bytes 6148 | tf_op jit(solution)/shard_map/while
  171.8 5.7 %copy-start.15 = (f32[1,512]{1,0:T(1,128)S(1)}, f32[1,512]{1,0:T(1,128)}, u32[]{:S(2)}) copy-start(f32[1,512]{1,0:T(1,128)} %get-tuple-element.1032) | copy-start | bytes 6148 | tf_op jit(solution)/shard_map/while
  182.6 5.7 %copy-start.5 = (f32[1,512]{1,0:T(1,128)S(1)}, f32[1,512]{1,0:T(1,128)}, u32[]{:S(2)}) copy-start(f32[1,512]{1,0:T(1,128)} %get-tuple-element.1028) | copy-start | bytes 6148 | tf_op jit(solution)/shard_map/while
  182.6 5.7 %copy-start.10 = (f32[512]{0:T(512)S(1)}, f32[512]{0:T(512)}, u32[]{:S(2)}) copy-start(f32[512]{0:T(512)} %get-tuple-element.1001) | copy-start | bytes 6148 | tf_op jit(solution)/shard_map/while
  182.7 5.7 %copy-start.11 = (f32[512]{0:T(512)S(1)}, f32[512]{0:T(512)}, u32[]{:S(2)}) copy-start(f32[512]{0:T(512)} %get-tuple-element.1002) | copy-start | bytes 6148 | tf_op jit(solution)/shard_map/while
  182.7 5.7 %copy-start.14 = (f32[512]{0:T(512)S(1)}, f32[512]{0:T(512)}, u32[]{:S(2)}) copy-start(f32[512]{0:T(512)} %get-tuple-element.1038) | copy-start | bytes 6148 | tf_op jit(solution)/shard_map/while
  182.7 5.7 %copy-start.15 = (f32[1,512]{1,0:T(1,128)S(1)}, f32[1,512]{1,0:T(1,128)}, u32[]{:S(2)}) copy-start(f32[1,512]{1,0:T(1,128)} %get-tuple-element.1032) | copy-start | bytes 6148 | tf_op jit(solution)/shard_map/while
  193.5 5.7 %copy-start.5 = (f32[1,512]{1,0:T(1,128)S(1)}, f32[1,512]{1,0:T(1,128)}, u32[]{:S(2)}) copy-start(f32[1,512]{1,0:T(1,128)} %get-tuple-element.1028) | copy-start | bytes 6148 | tf_op jit(solution)/shard_map/while
  193.5 5.7 %copy-start.10 = (f32[512]{0:T(512)S(1)}, f32[512]{0:T(512)}, u32[]{:S(2)}) copy-start(f32[512]{0:T(512)} %get-tuple-element.1001) | copy-start | bytes 6148 | tf_op jit(solution)/shard_map/while
  193.5 5.7 %copy-start.11 = (f32[512]{0:T(512)S(1)}, f32[512]{0:T(512)}, u32[]{:S(2)}) copy-start(f32[512]{0:T(512)} %get-tuple-element.1002) | copy-start | bytes 6148 | tf_op jit(solution)/shard_map/while
  193.5 5.7 %copy-start.14 = (f32[512]{0:T(512)S(1)}, f32[512]{0:T(512)}, u32[]{:S(2)}) copy-start(f32[512]{0:T(512)} %get-tuple-element.1038) | copy-start | bytes 6148 | tf_op jit(solution)/shard_map/while
  193.5 5.7 %copy-start.15 = (f32[1,512]{1,0:T(1,128)S(1)}, f32[1,512]{1,0:T(1,128)}, u32[]{:S(2)}) copy-start(f32[1,512]{1,0:T(1,128)} %get-tuple-element.1032) | copy-start | bytes 6148 | tf_op jit(solution)/shard_map/while
  226.1 5.7 %copy-start.5 = (f32[1,512]{1,0:T(1,128)S(1)}, f32[1,512]{1,0:T(1,128)}, u32[]{:S(2)}) copy-start(f32[1,512]{1,0:T(1,128)} %get-tuple-element.1028) | copy-start | bytes 6148 | tf_op jit(solution)/shard_map/while
  226.1 5.7 %copy-start.10 = (f32[512]{0:T(512)S(1)}, f32[512]{0:T(512)}, u32[]{:S(2)}) copy-start(f32[512]{0:T(512)} %get-tuple-element.1001) | copy-start | bytes 6148 | tf_op jit(solution)/shard_map/while
  226.1 5.7 %copy-start.11 = (f32[512]{0:T(512)S(1)}, f32[512]{0:T(512)}, u32[]{:S(2)}) copy-start(f32[512]{0:T(512)} %get-tuple-element.1002) | copy-start | bytes 6148 | tf_op jit(solution)/shard_map/while
  226.1 5.7 %copy-start.14 = (f32[512]{0:T(512)S(1)}, f32[512]{0:T(512)}, u32[]{:S(2)}) copy-start(f32[512]{0:T(512)} %get-tuple-element.1038) | copy-start | bytes 6148 | tf_op jit(solution)/shard_map/while
  226.1 5.7 %copy-start.15 = (f32[1,512]{1,0:T(1,128)S(1)}, f32[1,512]{1,0:T(1,128)}, u32[]{:S(2)}) copy-start(f32[1,512]{1,0:T(1,128)} %get-tuple-element.1032) | copy-start | bytes 6148 | tf_op jit(solution)/shard_map/while
  237.0 5.7 %copy-start.5 = (f32[1,512]{1,0:T(1,128)S(1)}, f32[1,512]{1,0:T(1,128)}, u32[]{:S(2)}) copy-start(f32[1,512]{1,0:T(1,128)} %get-tuple-element.1028) | copy-start | bytes 6148 | tf_op jit(solution)/shard_map/while
  237.0 5.7 %copy-start.10 = (f32[512]{0:T(512)S(1)}, f32[512]{0:T(512)}, u32[]{:S(2)}) copy-start(f32[512]{0:T(512)} %get-tuple-element.1001) | copy-start | bytes 6148 | tf_op jit(solution)/shard_map/while
  237.0 5.7 %copy-start.11 = (f32[512]{0:T(512)S(1)}, f32[512]{0:T(512)}, u32[]{:S(2)}) copy-start(f32[512]{0:T(512)} %get-tuple-element.1002) | copy-start | bytes 6148 | tf_op jit(solution)/shard_map/while
  237.0 5.7 %copy-start.14 = (f32[512]{0:T(512)S(1)}, f32[512]{0:T(512)}, u32[]{:S(2)}) copy-start(f32[512]{0:T(512)} %get-tuple-element.1038) | copy-start | bytes 6148 | tf_op jit(solution)/shard_map/while
  237.0 5.7 %copy-start.15 = (f32[1,512]{1,0:T(1,128)S(1)}, f32[1,512]{1,0:T(1,128)}, u32[]{:S(2)}) copy-start(f32[1,512]{1,0:T(1,128)} %get-tuple-element.1032) | copy-start | bytes 6148 | tf_op jit(solution)/shard_map/while
  258.7 5.7 %copy-start.5 = (f32[1,512]{1,0:T(1,128)S(1)}, f32[1,512]{1,0:T(1,128)}, u32[]{:S(2)}) copy-start(f32[1,512]{1,0:T(1,128)} %get-tuple-element.1028) | copy-start | bytes 6148 | tf_op jit(solution)/shard_map/while
  258.7 5.7 %copy-start.10 = (f32[512]{0:T(512)S(1)}, f32[512]{0:T(512)}, u32[]{:S(2)}) copy-start(f32[512]{0:T(512)} %get-tuple-element.1001) | copy-start | bytes 6148 | tf_op jit(solution)/shard_map/while
  258.7 5.7 %copy-start.11 = (f32[512]{0:T(512)S(1)}, f32[512]{0:T(512)}, u32[]{:S(2)}) copy-start(f32[512]{0:T(512)} %get-tuple-element.1002) | copy-start | bytes 6148 | tf_op jit(solution)/shard_map/while
  258.7 5.7 %copy-start.14 = (f32[512]{0:T(512)S(1)}, f32[512]{0:T(512)}, u32[]{:S(2)}) copy-start(f32[512]{0:T(512)} %get-tuple-element.1038) | copy-start | bytes 6148 | tf_op jit(solution)/shard_map/while
  258.8 5.7 %copy-start.15 = (f32[1,512]{1,0:T(1,128)S(1)}, f32[1,512]{1,0:T(1,128)}, u32[]{:S(2)}) copy-start(f32[1,512]{1,0:T(1,128)} %get-tuple-element.1032) | copy-start | bytes 6148 | tf_op jit(solution)/shard_map/while
  280.2 61.5 %copy-start.6 = (f32[512]{0:T(512)S(1)}, f32[512]{0:T(512)}, u32[]{:S(2)}) copy-start(f32[512]{0:T(512)} %custom-call) | copy-start | bytes 6148
  280.2 61.5 %copy-start.7 = (f32[512]{0:T(512)S(1)}, f32[512]{0:T(512)}, u32[]{:S(2)}) copy-start(f32[512]{0:T(512)} %custom-call.1) | copy-start | bytes 6148
  353.2 11.3 %copy-start.13 = (f32[512]{0:T(512)S(1)}, f32[512]{0:T(512)}, u32[]{:S(2)}) copy-start(f32[512]{0:T(512)} %param.22) | copy-start | bytes 6148
  (28 other events, 152.0 us)
Sparse Core Ops, SparseCore 0:
  11.0 89.7 all-gather.3
where the time goes:
time: 378 us; the launch traced here: 373 us
  matrix products  134 us (35%)
  waiting for transfers between devices  85.1 us (23%)
  blocking collectives  69.5 us (18%)
  local copies, waits for them, and re-layouts  43.1 us (11%)
  other arithmetic  22.5 us (6%)
  between operations  13.7 us (4%)
  loops' own time  5.22 us (1%)
    all_gather x1, waiting for transfers between devices, on_device(): lax.all_gather(normed, 'tp', axis=0, tiled=True)  85.1 us
    all_gather x1, blocking collectives, gathered_once(): both, at, found = (lax.all_gather(jnp.concatenate(lines), axis), 0, {})  60.4 us
    dot_general x16, matrix products, advance(): acc_im = jnp.dot(lower, w_im, precision=HIGHEST)  48.1 us
    dot_general x16, matrix products, advance(): acc_re = jnp.dot(lower, w_re, precision=HIGHEST)  32.4 us
    slice x32, local copies, waits for them, and re-layouts, advance(): ends = (cum_re[-1], cum_im[-1], full_re[-1], full_im[-1])  18.8 us
    dot_general x16, matrix products, advance(): in_im = jnp.dot(grouped, push_im, precision=HIGHEST)  15.3 us
    dot_general x16, matrix products, advance(): in_re = jnp.dot(grouped, push_re, precision=HIGHEST)  15.3 us
    dot_general x16, matrix products, advance(): elapsed = jnp.dot(lower, time_part, precision=HIGHEST)[:, None]  13.3 us
  transfers between devices with their start and end apart: 1, of which 1 were waited for; matrix products, arithmetic and copies ran while one was open for 1% of the time, Pallas kernels for 0%

commit v1 on v0

--- a/solution.py
+++ b/solution.py
@@ -6,6 +6,24 @@
 
 SPAN = 64
 HIGHEST = lax.Precision.HIGHEST
+
+
+def gather_around(shard, axis, dim):
+    ways, here, step = (lax.axis_size(axis), lax.axis_index(axis), shard.shape[dim])
+    shape = [n * ways if d == dim else n for d, n in enumerate(shard.shape)]
+    full = lax.dynamic_update_slice_in_dim(
+        jnp.zeros(shape, shard.dtype), shard, here * step, axis=dim
+    )
+    going_up = going_down = shard
+    for far in range(1, ways // 2 + 1):
+        going_up = lax.ppermute(going_up, axis, [(d, (d + 1) % ways) for d in range(ways)])
+        full = lax.dynamic_update_slice_in_dim(full, going_up, (here - far) % ways * step, axis=dim)
+        if 2 * far < ways:
+            going_down = lax.ppermute(going_down, axis, [(d, (d - 1) % ways) for d in range(ways)])
+            full = lax.dynamic_update_slice_in_dim(
+                full, going_down, (here + far) % ways * step, axis=dim
+            )
+    return full
 
 
 def gathered_once(array, axis):
@@ -124,9 +142,7 @@
     normed = rms_rows(tokens, in_gain)
     rates, freqs, maps, reads = (decay_rate, frequency, input_map, readout)
     drive = jnp.dot(
-        lax.all_gather(normed, "tp", axis=0, tiled=True),
-        in_proj,
-        preferred_element_type=jnp.float32,
+        gather_around(normed, "tp", 0), in_proj, preferred_element_type=jnp.float32
     ).astype(jnp.bfloat16)
     tables = block_tables(maps, reads)
     flat_rates = rates.reshape(-1)

time: 378 us -> 373 us (0.987)
  waiting for transfers between devices: 85.1 us -> 15.7 us
  blocking collectives: 69.5 us -> 119 us
  starting transfers between devices: 0.06 us -> 19.2 us
  between operations: 13.7 us -> 0.38 us
  local copies, waits for them, and re-layouts: 43.1 us -> 52.8 us
    all_gather x1 -> x0, waiting for transfers between devices: 85.1 us -> none  [on_device(): lax.all_gather(normed, 'tp', axis=0, tiled=True)]
    all_gather x1, blocking collectives: 60.4 us -> 110 us  [gathered_once(): both, at, found = (lax.all_gather(jnp.concatenate(lines), axis), 0, {})]
    ppermute x0 -> x3, starting transfers between devices: none -> 19.2 us  [the longest x2 15.7 us: gather_around(): lax.ppermute(going_up, axis, [(d, (d + 1) % ways) for d in range(ways)])]
    ppermute x0 -> x3, waiting for transfers between devices: none -> 15.7 us  [the longest x2 15.7 us: gather_around(): lax.ppermute(going_up, axis, [(d, (d + 1) % ways) for d in range(ways)])]
    dynamic_update_slice x0 -> x3, local copies, waits for them, and re-layouts: none -> 7.02 us  [the longest x2 4.66 us: gather_around(): lax.dynamic_update_slice_in_dim(full, going_up, (here - far) % ways * ste...]
  transfers between devices with their start and end apart: 1 -> 3, of which waited for: 1 -> 2; matrix products, arithmetic and copies ran while one was open for 1% -> 3% of each run, Pallas kernels for 0% -> 0%
where the time goes in v1:
time: 373 us; the launch traced here: 369 us
  matrix products  134 us (36%)
  blocking collectives  119 us (32%)
  local copies, waits for them, and re-layouts  52.8 us (14%)
  other arithmetic  21.7 us (6%)
  starting transfers between devices  19.2 us (5%)
  waiting for transfers between devices  15.7 us (4%)
  loops' own time  5.22 us (1%)
    all_gather x1, blocking collectives, gathered_once(): both, at, found = (lax.all_gather(jnp.concatenate(lines), axis), 0, {})  110 us
    dot_general x16, matrix products, advance(): acc_im = jnp.dot(lower, w_im, precision=HIGHEST)  48 us
    dot_general x16, matrix products, advance(): acc_re = jnp.dot(lower, w_re, precision=HIGHEST)  33.2 us
    slice x32, local copies, waits for them, and re-layouts, advance(): ends = (cum_re[-1], cum_im[-1], full_re[-1], full_im[-1])  19 us
    ppermute x2, waiting for transfers between devices, gather_around(): lax.ppermute(going_up, axis, [(d, (d + 1) % ways) for d in range(ways)])  15.7 us
    ppermute x2, starting transfers between devices, gather_around(): lax.ppermute(going_up, axis, [(d, (d + 1) % ways) for d in range(ways)])  15.7 us
    dot_general x16, matrix products, advance(): in_im = jnp.dot(grouped, push_im, precision=HIGHEST)  15.3 us
    dot_general x16, matrix products, advance(): in_re = jnp.dot(grouped, push_re, precision=HIGHEST)  15.3 us
  transfers between devices with their start and end apart: 3, of which 2 were waited for; matrix products, arithmetic and copies ran while one was open for 3% of the time, Pallas kernels for 0%

profile of v1, /device:TPU:33, one launch (start us, length us, event | category | flops | bytes accessed | tf_op | source)
XLA Modules:
  0.0 368.5 jit_solution(6470050445651395024)
XLA Ops:
  0.0 1.7 fusion.44
  1.7 2.5 broadcast_in_dim.39
  4.2 1.6 constant_dynamic-update-slice_fusion.3
  5.9 4.2 %collective-permute-start = (bf16[256,2048]{1,0:T(8,128)(2,1)}, bf16[256,2048]{1,0:T(8,128)(2,1)}, u32[]{:S(2)}, u32[]{:S(2)}) collective-permute-start(bf16[256,2048]{1,0:T(8,128)(2,1)} %get-tuple-element.651), channel_id=1, source_target_pairs={{0,1},{1,2},{2,3},{3,0},{4,5},{5,6},{6,7},{7,4},{8,9},{9,10},{10,1... | collective-permute-start | bytes 3145736 | tf_op jit(solution)/shard_map/ppermute | solution.py:19
  10.1 3.5 collective-permute-start.1
  16.5 7.6 %collective-permute-done = bf16[256,2048]{1,0:T(8,128)(2,1)} collective-permute-done((bf16[256,2048]{1,0:T(8,128)(2,1)}, bf16[256,2048]{1,0:T(8,128)(2,1)}, u32[]{:S(2)}, u32[]{:S(2)}) %collective-permute-start) | collective-permute-done | bytes 1048608 | tf_op jit(solution)/shard_map/ppermute | solution.py:19
  24.1 11.5 %collective-permute-start.2 = (bf16[256,2048]{1,0:T(8,128)(2,1)}, bf16[256,2048]{1,0:T(8,128)(2,1)}, u32[]{:S(2)}, u32[]{:S(2)}) collective-permute-start(bf16[256,2048]{1,0:T(8,128)(2,1)} %collective-permute-done), channel_id=1, source_target_pairs={{0,1},{1,2},{2,3},{3,0},{4,5},{5,6},{6,7},{7,4},{8,9},{9,10},{10,1... | collective-permute-start | bytes 3145736 | tf_op jit(solution)/shard_map/ppermute | solution.py:19
  37.6 2.3 constant_dynamic-update-slice_fusion.2
  40.0 2.4 constant_dynamic-update-slice_fusion.1
  42.3 8.2 %collective-permute-done.2 = bf16[256,2048]{1,0:T(8,128)(2,1)} collective-permute-done((bf16[256,2048]{1,0:T(8,128)(2,1)}, bf16[256,2048]{1,0:T(8,128)(2,1)}, u32[]{:S(2)}, u32[]{:S(2)}) %collective-permute-start.2) | collective-permute-done | bytes 1048608 | tf_op jit(solution)/shard_map/ppermute | solution.py:19
  50.5 2.3 constant_dynamic-update-slice_fusion
  52.8 4.1 %convolution_convert_fusion.1 = bf16[1024,128]{1,0:T(8,128)(2,1)} fusion(bf16[1024,2048]{1,0:T(8,128)(2,1)} %constant_dynamic-update-slice_fusion, bf16[2048,128]{1,0:T(8,128)(2,1)S(1)} %copy-done.18), kind=kOutput, calls=%fused_computation.81 | convolution fusion | flops 537001984 | bytes 4980736 | tf_op jit(solution)/shard_map/dot_general | solution.py:144
  58.1 174.6 %while.48 = (s32[]{:T(128)}, f32[512]{0:T(512)S(1)}, f32[512]{0:T(512)S(1)}, f32[512]{0:T(512)}, f32[512]{0:T(512)}, /*index=5*/f32[16,64,512]{2,1,0:T(8,128)}, ...) while((s32[]{:T(128)}, f32[512]{0:T(512)S(1)}, ...), condition=%wide.wide.region_2.3_spmd.clone.clone.clone, body=%wide.wide.region_1.2_spmd.clone.clone.clone.sunk | while | flops 153889792 | bytes 4405837 | solution.py:161
  62.1 2.1 convolution_bitcast_fusion.8
  64.3 3.0 add_dynamic-update-slice_fusion.3
  70.5 1.0 fusion.105
  73.0 2.1 convolution_bitcast_fusion.8
  75.2 3.0 add_dynamic-update-slice_fusion.3
  80.3 1.0 fusion.104
  83.9 2.1 convolution_bitcast_fusion.8
  86.1 3.0 add_dynamic-update-slice_fusion.3
  92.3 1.0 fusion.105
  94.8 2.1 convolution_bitcast_fusion.8
  97.0 3.0 add_dynamic-update-slice_fusion.3
  102.1 1.0 fusion.104
  105.8 2.1 convolution_bitcast_fusion.8
  107.9 3.0 add_dynamic-update-slice_fusion.3
  113.1 1.0 fusion.104
  116.7 2.1 convolution_bitcast_fusion.8
  118.8 3.0 add_dynamic-update-slice_fusion.3
  123.9 1.0 fusion.104
  127.5 2.1 convolution_bitcast_fusion.8
  129.7 3.0 add_dynamic-update-slice_fusion.3
  138.5 2.1 convolution_bitcast_fusion.8
  140.6 3.0 add_dynamic-update-slice_fusion.3
  145.8 1.0 fusion.104
  146.9 1.0 fusion.105
  149.4 2.1 convolution_bitcast_fusion.8
  151.5 3.0 add_dynamic-update-slice_fusion.3
  160.3 2.1 convolution_bitcast_fusion.8
  162.4 3.0 add_dynamic-update-slice_fusion.3
  167.6 1.0 fusion.104
  168.7 1.0 fusion.105
  171.2 2.1 convolution_bitcast_fusion.8
  173.4 3.0 add_dynamic-update-slice_fusion.3
  182.1 2.1 convolution_bitcast_fusion.8
  184.3 3.0 add_dynamic-update-slice_fusion.3
  193.0 2.1 convolution_bitcast_fusion.8
  195.2 3.0 add_dynamic-update-slice_fusion.3
  203.9 2.1 convolution_bitcast_fusion.8
  206.1 3.0 add_dynamic-update-slice_fusion.3
  212.4 1.0 fusion.105
  214.9 2.1 convolution_bitcast_fusion.8
  217.0 3.0 add_dynamic-update-slice_fusion.3
  222.1 1.0 fusion.104
  225.8 2.1 convolution_bitcast_fusion.8
  227.9 3.0 add_dynamic-update-slice_fusion.3
  233.4 110.3 %all-gather.1 = f32[64,4,512]{2,1,0:T(4,128)S(1)} all-gather(f32[1,4,512]{2,1,0:T(4,128)S(1)} %maximum_bitcast_fusion), channel_id=2, replica_groups=mesh['grp'=2,'sp'=64,'tp'=4] {'sp'}, dimensions={0}, use_global_device_ids=true | all-gather | bytes 532480 | tf_op jit(solution)/shard_map/all_gather | solution.py:37
  344.2 5.1 %while.47 = (s32[]{:T(128)}, f32[512]{0:T(512)S(1)}, f32[512]{0:T(512)S(1)}, s32[]{:T(128)}, f32[64,512]{1,0:T(8,128)S(1)}, /*index=5*/f32[64,512]{1,0:T(8,128)S...) while((s32[]{:T(128)}, f32[512]{0:T(512)S(1)}, f32[512]{0:T(512)S(1)}, ...), condition=%wide.region_4.5_spmd.clone, body=%wide.region_3.4_spmd.clone.sunk | while | flops 6148 | bytes 32897 | solution.py:57
  349.3 4.6 %multiply_add_fusion.5 = (f32[16,64,512]{2,1,0:T(8,128)S(1)}, f32[16,64,512]{2,1,0:T(8,128)S(1)}) fusion(f32[16,64,512]{2,1,0:T(8,128)} %get-tuple-element.435, f32[16,64,512]{2,1,0:T(8,128)} %get-tuple-element.437, f32[16,64,512]{2,1,0:T(8,128)} %get-tuple-element.429, f32[512]{0:T(512)S(1)} %get-tuple-element.436, f32[512]{0:T(512)S(1)} %get-tuple-element.434, ...), kind=kLoop, calls=%fused_computation.78 | loop fusion | flops 4194304 | bytes 12587008 | tf_op jit(solution)/shard_map/add | solution.py:174
  353.9 1.8 fusion.60
  355.7 1.8 fusion.54
  357.7 8.9 %all_to_all.13 = bf16[4,256,128]{1,2,0:T(8,128)(2,1)S(1)} all-to-all(bf16[4,256,128]{1,2,0:T(8,128)(2,1)S(1)} %copy.20), channel_id=1, replica_groups=mesh['grp'=2,'sp'=64,'tp'=4] {'tp'}, dimensions={0} | all-to-all | bytes 524288 | tf_op jit(solution)/shard_map/all_to_all | solution.py:176
  366.8 1.7 convolution_convert_fusion
  (608 shorter events, 89.4 us)
Async XLA Ops:
  0.0 366.8 %copy-start = (bf16[512,2048]{1,0:T(8,128)(2,1)S(1)}, bf16[512,2048]{1,0:T(8,128)(2,1)}, u32[]{:S(2)}) copy-start(bf16[512,2048]{1,0:T(8,128)(2,1)} %param.23) | copy-start | bytes 6291460
  4.2 9.5 %copy-start.9 = (f32[8,64]{1,0:T(8,128)S(1)}, f32[8,64]{1,0:T(8,128)}, u32[]{:S(2)}) copy-start(f32[8,64]{1,0:T(8,128)} %param.19) | copy-start | bytes 6148
  4.2 9.6 %copy-start.10 = (f32[8,64]{1,0:T(8,128)S(1)}, f32[8,64]{1,0:T(8,128)}, u32[]{:S(2)}) copy-start(f32[8,64]{1,0:T(8,128)} %param.18) | copy-start | bytes 6148
  4.2 11.6 %copy-start.14 = (f32[1024]{0:T(1024)S(1)}, f32[1024]{0:T(1024)}, u32[]{:S(2)}) copy-start(f32[1024]{0:T(1024)} %param.15) | copy-start | bytes 12292
  4.2 12.3 %copy-start.4 = (f32[2,8,16,64]{3,2,1,0:T(8,128)S(1)}, f32[2,8,16,64]{3,2,1,0:T(8,128)}, u32[]{:S(2)}) copy-start(f32[2,8,16,64]{3,2,1,0:T(8,128)} %param.21) | copy-start | bytes 196612
  5.9 31.7 %copy-start.5 = (f32[2,8,64,16]{2,3,1,0:T(8,128)S(1)}, f32[2,8,64,16]{2,3,1,0:T(8,128)}, u32[]{:S(2)}) copy-start(f32[2,8,64,16]{2,3,1,0:T(8,128)} %param.20) | copy-start | bytes 196612
  5.9 18.3 %collective-permute-start = (bf16[256,2048]{1,0:T(8,128)(2,1)}, bf16[256,2048]{1,0:T(8,128)(2,1)}, u32[]{:S(2)}, u32[]{:S(2)}) collective-permute-start(bf16[256,2048]{1,0:T(8,128)(2,1)} %get-tuple-element.651), channel_id=1, source_target_pairs={{0,1},{1,2},{2,3},{3,0},{4,5},{5,6},{6,7},{7,4},{8,9},{9,10},{10,1... | collective-permute-start | bytes 3145736 | tf_op jit(solution)/shard_map/ppermute | solution.py:19
  10.1 29.9 %collective-permute-start.1 = (bf16[256,2048]{1,0:T(8,128)(2,1)}, bf16[256,2048]{1,0:T(8,128)(2,1)}, u32[]{:S(2)}, u32[]{:S(2)}) collective-permute-start(bf16[256,2048]{1,0:T(8,128)(2,1)} %get-tuple-element.651), channel_id=1, source_target_pairs={{0,3},{1,0},{2,1},{3,2},{4,7},{5,4},{6,5},{7,6},{8,11},{9,8},{10,9... | collective-permute-start | bytes 3145736 | tf_op jit(solution)/shard_map/ppermute | solution.py:22
  24.1 26.3 %collective-permute-start.2 = (bf16[256,2048]{1,0:T(8,128)(2,1)}, bf16[256,2048]{1,0:T(8,128)(2,1)}, u32[]{:S(2)}, u32[]{:S(2)}) collective-permute-start(bf16[256,2048]{1,0:T(8,128)(2,1)} %collective-permute-done), channel_id=1, source_target_pairs={{0,1},{1,2},{2,3},{3,0},{4,5},{5,6},{6,7},{7,4},{8,9},{9,10},{10,1... | collective-permute-start | bytes 3145736 | tf_op jit(solution)/shard_map/ppermute | solution.py:19
  39.9 12.9 %copy-start.18 = (bf16[2048,128]{1,0:T(8,128)(2,1)S(1)}, bf16[2048,128]{1,0:T(8,128)(2,1)}, u32[]{:S(2)}) copy-start(bf16[2048,128]{1,0:T(8,128)(2,1)} %param.17) | copy-start | bytes 1572868
  91.2 5.8 %copy-start.6 = (f32[1,512]{1,0:T(1,128)S(1)}, f32[1,512]{1,0:T(1,128)}, u32[]{:S(2)}) copy-start(f32[1,512]{1,0:T(1,128)} %get-tuple-element.1030) | copy-start | bytes 6148 | tf_op jit(solution)/shard_map/while
  91.2 5.8 %copy-start.12 = (f32[512]{0:T(512)S(1)}, f32[512]{0:T(512)}, u32[]{:S(2)}) copy-start(f32[512]{0:T(512)} %get-tuple-element.1003) | copy-start | bytes 6148 | tf_op jit(solution)/shard_map/while
  91.2 5.8 %copy-start.13 = (f32[512]{0:T(512)S(1)}, f32[512]{0:T(512)}, u32[]{:S(2)}) copy-start(f32[512]{0:T(512)} %get-tuple-element.1004) | copy-start | bytes 6148 | tf_op jit(solution)/shard_map/while
  91.2 5.8 %copy-start.16 = (f32[512]{0:T(512)S(1)}, f32[512]{0:T(512)}, u32[]{:S(2)}) copy-start(f32[512]{0:T(512)} %get-tuple-element.1040) | copy-start | bytes 6148 | tf_op jit(solution)/shard_map/while
  91.2 5.8 %copy-start.17 = (f32[1,512]{1,0:T(1,128)S(1)}, f32[1,512]{1,0:T(1,128)}, u32[]{:S(2)}) copy-start(f32[1,512]{1,0:T(1,128)} %get-tuple-element.1034) | copy-start | bytes 6148 | tf_op jit(solution)/shard_map/while
  102.1 5.8 %copy-start.6 = (f32[1,512]{1,0:T(1,128)S(1)}, f32[1,512]{1,0:T(1,128)}, u32[]{:S(2)}) copy-start(f32[1,512]{1,0:T(1,128)} %get-tuple-element.1030) | copy-start | bytes 6148 | tf_op jit(solution)/shard_map/while
  102.1 5.8 %copy-start.12 = (f32[512]{0:T(512)S(1)}, f32[512]{0:T(512)}, u32[]{:S(2)}) copy-start(f32[512]{0:T(512)} %get-tuple-element.1003) | copy-start | bytes 6148 | tf_op jit(solution)/shard_map/while
  102.1 5.8 %copy-start.13 = (f32[512]{0:T(512)S(1)}, f32[512]{0:T(512)}, u32[]{:S(2)}) copy-start(f32[512]{0:T(512)} %get-tuple-element.1004) | copy-start | bytes 6148 | tf_op jit(solution)/shard_map/while
  102.1 5.8 %copy-start.16 = (f32[512]{0:T(512)S(1)}, f32[512]{0:T(512)}, u32[]{:S(2)}) copy-start(f32[512]{0:T(512)} %get-tuple-element.1040) | copy-start | bytes 6148 | tf_op jit(solution)/shard_map/while
  102.1 5.8 %copy-start.17 = (f32[1,512]{1,0:T(1,128)S(1)}, f32[1,512]{1,0:T(1,128)}, u32[]{:S(2)}) copy-start(f32[1,512]{1,0:T(1,128)} %get-tuple-element.1034) | copy-start | bytes 6148 | tf_op jit(solution)/shard_map/while
  123.9 5.8 %copy-start.6 = (f32[1,512]{1,0:T(1,128)S(1)}, f32[1,512]{1,0:T(1,128)}, u32[]{:S(2)}) copy-start(f32[1,512]{1,0:T(1,128)} %get-tuple-element.1030) | copy-start | bytes 6148 | tf_op jit(solution)/shard_map/while
  145.7 5.8 %copy-start.6 = (f32[1,512]{1,0:T(1,128)S(1)}, f32[1,512]{1,0:T(1,128)}, u32[]{:S(2)}) copy-start(f32[1,512]{1,0:T(1,128)} %get-tuple-element.1030) | copy-start | bytes 6148 | tf_op jit(solution)/shard_map/while
  145.7 5.8 %copy-start.12 = (f32[512]{0:T(512)S(1)}, f32[512]{0:T(512)}, u32[]{:S(2)}) copy-start(f32[512]{0:T(512)} %get-tuple-element.1003) | copy-start | bytes 6148 | tf_op jit(solution)/shard_map/while
  145.7 5.8 %copy-start.13 = (f32[512]{0:T(512)S(1)}, f32[512]{0:T(512)}, u32[]{:S(2)}) copy-start(f32[512]{0:T(512)} %get-tuple-element.1004) | copy-start | bytes 6148 | tf_op jit(solution)/shard_map/while
  145.7 5.8 %copy-start.16 = (f32[512]{0:T(512)S(1)}, f32[512]{0:T(512)}, u32[]{:S(2)}) copy-start(f32[512]{0:T(512)} %get-tuple-element.1040) | copy-start | bytes 6148 | tf_op jit(solution)/shard_map/while
  145.8 5.8 %copy-start.17 = (f32[1,512]{1,0:T(1,128)S(1)}, f32[1,512]{1,0:T(1,128)}, u32[]{:S(2)}) copy-start(f32[1,512]{1,0:T(1,128)} %get-tuple-element.1034) | copy-start | bytes 6148 | tf_op jit(solution)/shard_map/while
  156.6 5.8 %copy-start.6 = (f32[1,512]{1,0:T(1,128)S(1)}, f32[1,512]{1,0:T(1,128)}, u32[]{:S(2)}) copy-start(f32[1,512]{1,0:T(1,128)} %get-tuple-element.1030) | copy-start | bytes 6148 | tf_op jit(solution)/shard_map/while
  156.6 5.8 %copy-start.12 = (f32[512]{0:T(512)S(1)}, f32[512]{0:T(512)}, u32[]{:S(2)}) copy-start(f32[512]{0:T(512)} %get-tuple-element.1003) | copy-start | bytes 6148 | tf_op jit(solution)/shard_map/while
  156.6 5.8 %copy-start.13 = (f32[512]{0:T(512)S(1)}, f32[512]{0:T(512)}, u32[]{:S(2)}) copy-start(f32[512]{0:T(512)} %get-tuple-element.1004) | copy-start | bytes 6148 | tf_op jit(solution)/shard_map/while
  156.7 5.8 %copy-start.16 = (f32[512]{0:T(512)S(1)}, f32[512]{0:T(512)}, u32[]{:S(2)}) copy-start(f32[512]{0:T(512)} %get-tuple-element.1040) | copy-start | bytes 6148 | tf_op jit(solution)/shard_map/while
  156.7 5.8 %copy-start.17 = (f32[1,512]{1,0:T(1,128)S(1)}, f32[1,512]{1,0:T(1,128)}, u32[]{:S(2)}) copy-start(f32[1,512]{1,0:T(1,128)} %get-tuple-element.1034) | copy-start | bytes 6148 | tf_op jit(solution)/shard_map/while
  167.5 5.8 %copy-start.6 = (f32[1,512]{1,0:T(1,128)S(1)}, f32[1,512]{1,0:T(1,128)}, u32[]{:S(2)}) copy-start(f32[1,512]{1,0:T(1,128)} %get-tuple-element.1030) | copy-start | bytes 6148 | tf_op jit(solution)/shard_map/while
  167.5 5.8 %copy-start.12 = (f32[512]{0:T(512)S(1)}, f32[512]{0:T(512)}, u32[]{:S(2)}) copy-start(f32[512]{0:T(512)} %get-tuple-element.1003) | copy-start | bytes 6148 | tf_op jit(solution)/shard_map/while
  167.6 5.8 %copy-start.13 = (f32[512]{0:T(512)S(1)}, f32[512]{0:T(512)}, u32[]{:S(2)}) copy-start(f32[512]{0:T(512)} %get-tuple-element.1004) | copy-start | bytes 6148 | tf_op jit(solution)/shard_map/while
  167.6 5.8 %copy-start.16 = (f32[512]{0:T(512)S(1)}, f32[512]{0:T(512)}, u32[]{:S(2)}) copy-start(f32[512]{0:T(512)} %get-tuple-element.1040) | copy-start | bytes 6148 | tf_op jit(solution)/shard_map/while
  167.6 5.8 %copy-start.17 = (f32[1,512]{1,0:T(1,128)S(1)}, f32[1,512]{1,0:T(1,128)}, u32[]{:S(2)}) copy-start(f32[1,512]{1,0:T(1,128)} %get-tuple-element.1034) | copy-start | bytes 6148 | tf_op jit(solution)/shard_map/while
  178.5 5.8 %copy-start.6 = (f32[1,512]{1,0:T(1,128)S(1)}, f32[1,512]{1,0:T(1,128)}, u32[]{:S(2)}) copy-start(f32[1,512]{1,0:T(1,128)} %get-tuple-element.1030) | copy-start | bytes 6148 | tf_op jit(solution)/shard_map/while
  178.5 5.8 %copy-start.12 = (f32[512]{0:T(512)S(1)}, f32[512]{0:T(512)}, u32[]{:S(2)}) copy-start(f32[512]{0:T(512)} %get-tuple-element.1003) | copy-start | bytes 6148 | tf_op jit(solution)/shard_map/while
  178.5 5.8 %copy-start.13 = (f32[512]{0:T(512)S(1)}, f32[512]{0:T(512)}, u32[]{:S(2)}) copy-start(f32[512]{0:T(512)} %get-tuple-element.1004) | copy-start | bytes 6148 | tf_op jit(solution)/shard_map/while
  178.5 5.8 %copy-start.16 = (f32[512]{0:T(512)S(1)}, f32[512]{0:T(512)}, u32[]{:S(2)}) copy-start(f32[512]{0:T(512)} %get-tuple-element.1040) | copy-start | bytes 6148 | tf_op jit(solution)/shard_map/while
  178.5 5.8 %copy-start.17 = (f32[1,512]{1,0:T(1,128)S(1)}, f32[1,512]{1,0:T(1,128)}, u32[]{:S(2)}) copy-start(f32[1,512]{1,0:T(1,128)} %get-tuple-element.1034) | copy-start | bytes 6148 | tf_op jit(solution)/shard_map/while
  189.4 5.8 %copy-start.6 = (f32[1,512]{1,0:T(1,128)S(1)}, f32[1,512]{1,0:T(1,128)}, u32[]{:S(2)}) copy-start(f32[1,512]{1,0:T(1,128)} %get-tuple-element.1030) | copy-start | bytes 6148 | tf_op jit(solution)/shard_map/while
  189.4 5.8 %copy-start.12 = (f32[512]{0:T(512)S(1)}, f32[512]{0:T(512)}, u32[]{:S(2)}) copy-start(f32[512]{0:T(512)} %get-tuple-element.1003) | copy-start | bytes 6148 | tf_op jit(solution)/shard_map/while
  189.4 5.8 %copy-start.13 = (f32[512]{0:T(512)S(1)}, f32[512]{0:T(512)}, u32[]{:S(2)}) copy-start(f32[512]{0:T(512)} %get-tuple-element.1004) | copy-start | bytes 6148 | tf_op jit(solution)/shard_map/while
  189.4 5.8 %copy-start.16 = (f32[512]{0:T(512)S(1)}, f32[512]{0:T(512)}, u32[]{:S(2)}) copy-start(f32[512]{0:T(512)} %get-tuple-element.1040) | copy-start | bytes 6148 | tf_op jit(solution)/shard_map/while
  189.4 5.8 %copy-start.17 = (f32[1,512]{1,0:T(1,128)S(1)}, f32[1,512]{1,0:T(1,128)}, u32[]{:S(2)}) copy-start(f32[1,512]{1,0:T(1,128)} %get-tuple-element.1034) | copy-start | bytes 6148 | tf_op jit(solution)/shard_map/while
  200.3 5.8 %copy-start.6 = (f32[1,512]{1,0:T(1,128)S(1)}, f32[1,512]{1,0:T(1,128)}, u32[]{:S(2)}) copy-start(f32[1,512]{1,0:T(1,128)} %get-tuple-element.1030) | copy-start | bytes 6148 | tf_op jit(solution)/shard_map/while
  200.3 5.8 %copy-start.12 = (f32[512]{0:T(512)S(1)}, f32[512]{0:T(512)}, u32[]{:S(2)}) copy-start(f32[512]{0:T(512)} %get-tuple-element.1003) | copy-start | bytes 6148 | tf_op jit(solution)/shard_map/while
  200.3 5.8 %copy-start.13 = (f32[512]{0:T(512)S(1)}, f32[512]{0:T(512)}, u32[]{:S(2)}) copy-start(f32[512]{0:T(512)} %get-tuple-element.1004) | copy-start | bytes 6148 | tf_op jit(solution)/shard_map/while
  200.3 5.8 %copy-start.16 = (f32[512]{0:T(512)S(1)}, f32[512]{0:T(512)}, u32[]{:S(2)}) copy-start(f32[512]{0:T(512)} %get-tuple-element.1040) | copy-start | bytes 6148 | tf_op jit(solution)/shard_map/while
  200.3 5.8 %copy-start.17 = (f32[1,512]{1,0:T(1,128)S(1)}, f32[1,512]{1,0:T(1,128)}, u32[]{:S(2)}) copy-start(f32[1,512]{1,0:T(1,128)} %get-tuple-element.1034) | copy-start | bytes 6148 | tf_op jit(solution)/shard_map/while
  211.2 5.8 %copy-start.6 = (f32[1,512]{1,0:T(1,128)S(1)}, f32[1,512]{1,0:T(1,128)}, u32[]{:S(2)}) copy-start(f32[1,512]{1,0:T(1,128)} %get-tuple-element.1030) | copy-start | bytes 6148 | tf_op jit(solution)/shard_map/while
  211.2 5.8 %copy-start.12 = (f32[512]{0:T(512)S(1)}, f32[512]{0:T(512)}, u32[]{:S(2)}) copy-start(f32[512]{0:T(512)} %get-tuple-element.1003) | copy-start | bytes 6148 | tf_op jit(solution)/shard_map/while
  211.2 5.8 %copy-start.13 = (f32[512]{0:T(512)S(1)}, f32[512]{0:T(512)}, u32[]{:S(2)}) copy-start(f32[512]{0:T(512)} %get-tuple-element.1004) | copy-start | bytes 6148 | tf_op jit(solution)/shard_map/while
  211.2 5.8 %copy-start.16 = (f32[512]{0:T(512)S(1)}, f32[512]{0:T(512)}, u32[]{:S(2)}) copy-start(f32[512]{0:T(512)} %get-tuple-element.1040) | copy-start | bytes 6148 | tf_op jit(solution)/shard_map/while
  211.2 5.8 %copy-start.17 = (f32[1,512]{1,0:T(1,128)S(1)}, f32[1,512]{1,0:T(1,128)}, u32[]{:S(2)}) copy-start(f32[1,512]{1,0:T(1,128)} %get-tuple-element.1034) | copy-start | bytes 6148 | tf_op jit(solution)/shard_map/while
  222.1 5.8 %copy-start.6 = (f32[1,512]{1,0:T(1,128)S(1)}, f32[1,512]{1,0:T(1,128)}, u32[]{:S(2)}) copy-start(f32[1,512]{1,0:T(1,128)} %get-tuple-element.1030) | copy-start | bytes 6148 | tf_op jit(solution)/shard_map/while
  222.1 5.8 %copy-start.12 = (f32[512]{0:T(512)S(1)}, f32[512]{0:T(512)}, u32[]{:S(2)}) copy-start(f32[512]{0:T(512)} %get-tuple-element.1003) | copy-start | bytes 6148 | tf_op jit(solution)/shard_map/while
  222.1 5.8 %copy-start.13 = (f32[512]{0:T(512)S(1)}, f32[512]{0:T(512)}, u32[]{:S(2)}) copy-start(f32[512]{0:T(512)} %get-tuple-element.1004) | copy-start | bytes 6148 | tf_op jit(solution)/shard_map/while
  222.1 5.8 %copy-start.16 = (f32[512]{0:T(512)S(1)}, f32[512]{0:T(512)}, u32[]{:S(2)}) copy-start(f32[512]{0:T(512)} %get-tuple-element.1040) | copy-start | bytes 6148 | tf_op jit(solution)/shard_map/while
  222.1 5.8 %copy-start.17 = (f32[1,512]{1,0:T(1,128)S(1)}, f32[1,512]{1,0:T(1,128)}, u32[]{:S(2)}) copy-start(f32[1,512]{1,0:T(1,128)} %get-tuple-element.1034) | copy-start | bytes 6148 | tf_op jit(solution)/shard_map/while
  232.7 111.4 %copy-start.7 = (f32[512]{0:T(512)S(1)}, f32[512]{0:T(512)}, u32[]{:S(2)}) copy-start(f32[512]{0:T(512)} %custom-call) | copy-start | bytes 6148
  232.7 111.4 %copy-start.8 = (f32[512]{0:T(512)S(1)}, f32[512]{0:T(512)}, u32[]{:S(2)}) copy-start(f32[512]{0:T(512)} %custom-call.1) | copy-start | bytes 6148
  355.7 11.0 %copy-start.15 = (f32[512]{0:T(512)S(1)}, f32[512]{0:T(512)}, u32[]{:S(2)}) copy-start(f32[512]{0:T(512)} %param.22) | copy-start | bytes 6148
  (33 other events, 178.6 us)
